TPU v7x, 32 devices: a whole 2x2x4 slice. The times are simulated.
32 devices in a mesh: fs: 8 (over z, x), tp: 4 (over y, core).
Axes of the slice: x: 2, y: 2, z: 4, core: 2. Of those that a mesh axis runs over, the one named last changes fastest.
Arguments:
- tokens: bfloat16 [1024, 2048], P('fs'), may hold values from -6 to 6
- route_ids: int32 [1024, 2], P('fs'), may hold values from 0 to 15, as said below
- route_weights: float32 [1024, 2], P('fs'), may hold values from 0.05 to 0.6
- norm_gain: float32 [2048], P('fs'), may hold values from 0.1 to 1.9
- gate_weight: float32 [16, 2048, 1024], P(None, 'fs', 'tp'), may hold values from -6 to 6
- up_weight: float32 [16, 2048, 1024], P(None, 'fs', 'tp'), may hold values from -6 to 6
- down_weight: float32 [16, 2048, 1024], P(None, 'fs', 'tp'), may hold values from -6 to 6
Outputs:
- gate_served: bfloat16 [16, 2048, 1024], P('fs', None, 'tp')
- up_served: bfloat16 [16, 2048, 1024], P('fs', None, 'tp')
- down_served: bfloat16 [16, 2048, 1024], P('fs', None, 'tp')
- combined: bfloat16 [1024, 2048], P('fs', 'tp')
Inputs may be any that keep to these rules, and one draw needn't show every extreme that they name: `route_ids`: each row names 2 different experts of one group, numbers g * 4 to g * 4 + 3 for some g. In each aligned block of 128 rows (the rows of one index of fs) no expert is named by more than 32 rows, and some experts are named by exactly 32 rows in every block.
All inputs are finite; a program needn't handle non-finite values.
Results may differ from a plain program's by a relative error of at most 0.015.
Values may be sent and summed in bfloat16 or wider, within the bound.
A program may use at most 64 MiB of HBM per device.

v0:
```python
import functools

import jax
import jax.numpy as jnp
from jax import lax
from jax.experimental import pallas as pl
from jax.experimental.pallas import tpu as pltpu
from jax.sharding import PartitionSpec as P

GROUPS = 4
EPSILON = 1e-06
MESH = pl.DeviceIdType.MESH
LAG = 2
F32, BF16, I32 = jnp.float32, jnp.bfloat16, jnp.int32


def matmul(a, b, contract=((1,), (0,))):
    return lax.dot_general(a, b, (contract, ((), ())), preferred_element_type=F32)


def assignment(ids_t, experts, cap):
    n_tok = ids_t.shape[1]
    slot = lax.broadcasted_iota(I32, (experts * cap, n_tok), 0)
    first, second = ids_t[0:1, :] == slot // cap, ids_t[1:2, :] == slot // cap
    earlier = (
        lax.broadcasted_iota(I32, (n_tok, n_tok), 0) < lax.broadcasted_iota(I32, (n_tok, n_tok), 1)
    )
    named = (first | second).astype(F32).astype(BF16)
    place = matmul(named, earlier.astype(F32).astype(BF16))
    return (first | second) & (place.astype(I32) == slot % cap), first


def kernel(
    nf, nt,
    tokens, ids_t, gain, gate, up, down,
    gate_out, up_out, down_out, ret,
    wf, ws, xs, xr, hs, ps, pr, rs,
    load_sem, wsend, wrecv, xsend, xrecv, gsend, grecv, psend, precv, rsend, rrecv,
):
    f, t = lax.axis_index("fs"), lax.axis_index("tp")
    experts, rows, hidden = gate.shape
    n_tok, d_model = tokens.shape
    per = experts // nf
    cap = n_tok * GROUPS // experts
    cols = d_model // nt
    slots = experts * cap
    per_owner = cols // rows
    served = (gate_out, up_out, down_out)
    low_half = f < nf // 2

    def peer(k):
        down_to = jnp.where(k < nf - f, nf - k, nf - 1 - k)
        up_to = jnp.where(k <= f, k - 1, k)
        return jnp.where(k == 0, f, jnp.where(low_half, down_to, up_to))

    def other(k):
        return lax.rem(t + k, nt)

    def loads(e, a, k):
        n = peer(k) * per + e
        return pltpu.make_async_copy(
            (gate, up, down)[a].at[n], wf.at[a, n], load_sem.at[e, a, k]
        )

    def weight_copy(e, a, p, source):
        return pltpu.make_async_remote_copy(
            src_ref=ws.at[a, p * per + e],
            dst_ref=served[a].at[e, pl.ds(pl.multiple_of(source * rows, rows), rows), :],
            send_sem=wsend.at[e, a, p],
            recv_sem=wrecv.at[e, a, source],
            device_id={"fs": p},
            device_id_type=MESH,
        )

    def token_copy(p, source):
        return pltpu.make_async_remote_copy(
            src_ref=xs.at[pl.ds(p * per, per)],
            dst_ref=xr.at[t, :, pl.ds(pl.multiple_of(source * cap, cap), cap), :],
            send_sem=xsend.at[p],
            recv_sem=xrecv.at[source],
            device_id={"fs": p},
            device_id_type=MESH,
        )

    def gather_copy(o, source):
        return pltpu.make_async_remote_copy(
            src_ref=xr.at[source],
            dst_ref=xr.at[source],
            send_sem=gsend.at[o],
            recv_sem=grecv.at[source],
            device_id={"tp": o},
            device_id_type=MESH,
        )

    def partial_copy(e, s, source):
        return pltpu.make_async_remote_copy(
            src_ref=ps.at[e, s],
            dst_ref=pr.at[source, e, lax.rem(s, per_owner)],
            send_sem=psend.at[e, s],
            recv_sem=precv.at[source, e, lax.rem(s, per_owner)],
            device_id={"tp": s // per_owner},
            device_id_type=MESH,
        )

    def return_copy(e, p, source, i):
        return pltpu.make_async_remote_copy(
            src_ref=rs.at[e, i, pl.ds(pl.multiple_of(p * cap, cap), cap), :],
            dst_ref=ret.at[i, source * per + e],
            send_sem=rsend.at[e, i, p],
            recv_sem=rrecv.at[e, i, source],
            device_id={"fs": p},
            device_id_type=MESH,
        )

    def each(first, last, action):
        def go(k, carry):
            action(k)
            return carry
        lax.fori_loop(first, last, go, 0)

    each(1, nf, lambda k: loads(0, 0, k).start())
    loads(0, 0, 0).start()

    barrier = pltpu.get_barrier_semaphore()
    each(1, nf, lambda k: pl.semaphore_signal(
        barrier, inc=1, device_id={"fs": peer(k)}, device_id_type=MESH))
    each(1, nt, lambda k: pl.semaphore_signal(
        barrier, inc=1, device_id={"tp": other(k)}, device_id_type=MESH))
    pl.semaphore_wait(barrier, nf + nt - 2)

    square = lax.broadcasted_iota(I32, (rows, rows), 0) == lax.broadcasted_iota(I32, (rows, rows), 1)
    gain_column = jnp.sum(jnp.where(square, gain[...], 0.0), axis=1, keepdims=True)

    def converted(a, n):
        value = wf[a, n]
        if a < 2:
            value = value * gain_column
        return value.astype(BF16)

    def send_weights(e, a):
        e_next, a_next = (e, a + 1) if a < 2 else (e + 1, 0)

        def load_next(k):
            if e_next < per:
                loads(e_next, a_next, k).start()

        def one(k):
            p = peer(k)
            loads(e, a, k).wait()
            load_next(k)
            ws[a, p * per + e] = converted(a, p * per + e)
            weight_copy(e, a, p, f).start()
        each(1, nf, one)
        loads(e, a, 0).wait()
        load_next(0)
        served[a][e, pl.ds(pl.multiple_of(f * rows, rows), rows), :] = converted(a, f * per + e)

    send_weights(0, 0)

    wide = tokens[...].astype(F32)
    scale = lax.rsqrt(jnp.mean(wide * wide, axis=1, keepdims=True) + EPSILON)
    own = tokens[:, pl.ds(pl.multiple_of(t * cols, cols), cols)].astype(F32)
    normed = (own * scale).astype(BF16)
    chosen, _ = assignment(ids_t, experts, cap)
    picked = matmul(chosen.astype(F32).astype(BF16), normed)
    xs[...] = picked.reshape(experts, cap, cols).astype(BF16)
    each(1, nf, lambda k: token_copy(peer(k), f).start())
    own_rows = pl.ds(pl.multiple_of(f * cap, cap), cap)
    xr[t, :, own_rows, :] = xs[pl.ds(f * per, per)]

    for e in range(per):
        for a in range(3):
            if e + a > 0:
                send_weights(e, a)

    each(1, nf, lambda k: token_copy(f, peer(k)).wait_recv())
    each(1, nt, lambda k: gather_copy(other(k), t).start())
    each(1, nt, lambda k: gather_copy(t, other(k)).wait_recv())

    def product(a, e):
        total = jnp.zeros((nf * cap, hidden), F32)
        for o in range(nt):
            total += matmul(xr[o, e], served[a][e, o * cols:(o + 1) * cols, :])
        return total * d_model ** (-0.5)

    hidden_scale = (hidden * nt) ** (-0.5)

    def block_at(j):
        return jnp.where(low_half, j, nf - 1 - j)

    def block(e, j):
        s = block_at(j)

        @pl.when(s != f)
        def _():
            weight_copy(e, 2, f, s).wait_recv()
        tile = down_out[e, pl.ds(pl.multiple_of(s * rows, rows), rows), :]
        ps[e, s] = (matmul(hs[...], tile, ((1,), (1,))) * hidden_scale).astype(BF16)

        @pl.when(s // per_owner != t)
        def _():
            partial_copy(e, s, t).start()

    def finish(e, j):
        s = block_at(j)
        i = lax.rem(s, per_owner)

        @pl.when(s // per_owner == t)
        def _():
            each(1, nt, lambda k: partial_copy(e, s, other(k)).wait_recv())
            total = ps[e, s].astype(F32)
            for k in range(1, nt):
                total += pr[other(k), e, i].astype(F32)
            rs[e, i] = total.astype(BF16)
            each(1, nf, lambda k: return_copy(e, peer(k), f, i).start())
            ret[i, f * per + e] = rs[e, i, own_rows, :]

    for e in range(per):
        each(1, nf, lambda k: weight_copy(e, 0, f, peer(k)).wait_recv())
        v = product(0, e)
        each(1, nf, lambda k: weight_copy(e, 1, f, peer(k)).wait_recv())
        hs[...] = (v / (1.0 + jnp.exp(-v)) * product(1, e)).astype(BF16)

        each(0, LAG, lambda j: block(e, j))

        def both(j):
            block(e, j)
            finish(e, j - LAG)
        each(LAG, nf, both)
        each(nf - LAG, nf, lambda j: finish(e, j))
    for e in range(per):
        each(0, per_owner, lambda i: each(
            1, nf, lambda k: return_copy(e, f, peer(k), i).wait_recv()))

    def drain(k):
        p = peer(k)
        for e in range(per):
            for a in range(3):
                weight_copy(e, a, p, f).wait_send()
            each(0, per_owner, lambda i: return_copy(e, p, f, i).wait_send())
        token_copy(p, f).wait_send()
    each(1, nf, drain)
    each(1, nt, lambda k: gather_copy(other(k), t).wait_send())

    def drain_partial(s):
        @pl.when(s // per_owner != t)
        def _():
            for e in range(per):
                partial_copy(e, s, t).wait_send()
    each(0, nf, drain_partial)


def finish_kernel(
    ids_t, weights_t, ret, gate, up, down, gate_out, up_out, down_out, combined, sem
):
    outs = [
        pltpu.make_async_copy(source, target, sem.at[a])
        for a, (source, target) in enumerate(((gate, gate_out), (up, up_out), (down, down_out)))
    ]
    for copy in outs:
        copy.start()
    chunks, experts, cap, width = ret.shape
    chosen, first = assignment(ids_t, experts, cap)
    share = jnp.where(chosen, jnp.where(first, weights_t[0:1, :], weights_t[1:2, :]), 0.0).T
    high = share.astype(BF16)
    low = (share - high.astype(F32)).astype(BF16)
    for i in range(chunks):
        back = ret[i].astype(F32).reshape(experts * cap, width).astype(BF16)
        value = matmul(high, back) + matmul(low, back)
        combined[:, i * width:(i + 1) * width] = value.astype(BF16)
    for copy in outs:
        copy.wait()


def body(nf, nt, tokens, route_ids, route_weights, norm_gain, gate_weight, up_weight, down_weight):
    experts, rows, hidden = gate_weight.shape
    n_tok, d_model = tokens.shape
    per = experts // nf
    cap = n_tok * GROUPS // experts
    cols = d_model // nt
    shape = (per, nf * rows, hidden)
    vmem, anywhere = pl.BlockSpec(memory_space=pltpu.VMEM), pl.BlockSpec(memory_space=pl.ANY)
    dma = pltpu.SemaphoreType.DMA
    per_owner = cols // rows
    ids_t, weights_t = route_ids.T, route_weights.T
    *served, ret = pl.pallas_call(
        functools.partial(kernel, nf, nt),
        out_shape=[pltpu.VMEM(shape, BF16)] * 3 + [pltpu.VMEM((per_owner, experts, cap, rows), BF16)],
        in_specs=[vmem] * 3 + [anywhere] * 3,
        out_specs=[vmem] * 4,
        scratch_shapes=[
            pltpu.VMEM((3, experts, rows, hidden), F32),
            pltpu.VMEM((3, experts, rows, hidden), BF16),
            pltpu.VMEM((experts, cap, cols), BF16),
            pltpu.VMEM((nt, per, nf * cap, cols), BF16),
            pltpu.VMEM((nf * cap, hidden), BF16),
            pltpu.VMEM((per, nf, nf * cap, rows), BF16),
            pltpu.VMEM((nt, per, per_owner, nf * cap, rows), BF16),
            pltpu.VMEM((per, per_owner, nf * cap, rows), BF16),
            dma((per, 3, nf)),
            dma((per, 3, nf)), dma((per, 3, nf)),
            dma((nf,)), dma((nf,)),
            dma((nt,)), dma((nt,)),
            dma((per, nf)), dma((nt, per, per_owner)),
            dma((per, per_owner, nf)), dma((per, per_owner, nf)),
        ],
        compiler_params=pltpu.CompilerParams(
            collective_id=0, has_side_effects=True, vmem_limit_bytes=54 * 1024 * 1024
        ),
    )(tokens, ids_t, norm_gain[None, :], gate_weight, up_weight, down_weight)
    out = jax.ShapeDtypeStruct(shape, BF16)
    return pl.pallas_call(
        finish_kernel,
        out_shape=(out, out, out, jax.ShapeDtypeStruct((n_tok, cols), BF16)),
        in_specs=[vmem] * 6,
        out_specs=(anywhere, anywhere, anywhere, vmem),
        scratch_shapes=[dma((3,))],
        compiler_params=pltpu.CompilerParams(vmem_limit_bytes=16 * 1024 * 1024),
    )(ids_t, weights_t, ret, *served)


def solution(mesh):
    split = P(None, "fs", "tp")
    served = P("fs", None, "tp")
    return jax.shard_map(
        functools.partial(body, mesh.shape["fs"], mesh.shape["tp"]),
        mesh=mesh,
        in_specs=(P("fs", None), P("fs", None), P("fs", None), P("fs"), split, split, split),
        out_specs=(served, served, served, P("fs", "tp")),
        check_vma=False,
    )
```

profile of v0, /device:TPU:0, one launch (start us, length us, event | category | flops | bytes accessed | tf_op | source)
XLA Modules:
  0.0 181.6 jit_solution(17435238188639039778)
XLA Ops:
  0.6 0.0 copy-start
  0.6 0.0 copy-start.1
  0.7 177.5 %shard_map.102 = (bf16[2,2048,256]{2,1,0:T(8,128)(2,1)S(1)}, bf16[2,2048,256]{2,1,0:T(8,128)(2,1)S(1)}, bf16[2,2048,256]{2,1,0:T(8,128)(2,1)S(1)}, bf16[2,16,32,256]{3,2,1,0:T(8,128)(2,1)S(1)}) custom-call(bf16[128,2048]{1,0:T(8,128)(2,1)} %tokens.1, s32[2,128]{1,0:T(2,128)} %bitcast.3, f32[1,256]{1,0:T(1,128)} %bitcast.6, f32[16,256,256]{2,1,0:T(8,128)} %gate.1, ...), custom_call_target="tpu_custom_call" | custom-call | tf_op jit(solution)/shard_map/pallas_call | solution.py:286
  178.1 0.0 copy-done
  178.2 0.0 copy-done.1
  178.2 3.5 %shard_map.103 = (bf16[2,2048,256]{2,1,0:T(8,128)(2,1)}, bf16[2,2048,256]{2,1,0:T(8,128)(2,1)}, bf16[2,2048,256]{2,1,0:T(8,128)(2,1)}, bf16[128,512]{1,0:T(8,128)(2,1)}) custom-call(s32[2,128]{1,0:T(2,128)S(1)} %bitcast.4, f32[2,128]{1,0:T(2,128)S(1)} %bitcast.5, bf16[2,16,32,256]{3,2,1,0:T(8,128)(2,1)S(1)} %get-tuple-element.8.ret, ...), custom_call_target="tpu_custom_call" | custom-call | tf_op jit(solution)/shard_map/pallas_call | solution.py:312
Async XLA Ops:
  0.6 177.5 %copy-start = (s32[128,2]{0,1:T(2,128)S(1)}, s32[128,2]{0,1:T(2,128)}, u32[]{:S(2)}) copy-start(s32[128,2]{0,1:T(2,128)} %param.8) | copy-start | bytes 3076
  0.6 177.5 %copy-start.1 = (f32[128,2]{0,1:T(2,128)S(1)}, f32[128,2]{0,1:T(2,128)}, u32[]{:S(2)}) copy-start(f32[128,2]{0,1:T(2,128)} %param.9) | copy-start | bytes 3076
where the time goes:
time: 182 us
  Pallas kernels  181 us (99%)
    pallas_call x1, Pallas kernels, body(): pl.pallas_call(functools.partial(kernel, nf, nt), out_shape=[pltpu.VMEM(s...  177 us

commit v1 on v0

v1 whole, which is shorter than its diff:
```python
import functools

import jax
import jax.numpy as jnp
from jax import lax
from jax.experimental import pallas as pl
from jax.experimental.pallas import tpu as pltpu
from jax.sharding import PartitionSpec as P

GROUPS = 4
EPSILON = 1e-06
MESH = pl.DeviceIdType.MESH
LAG = 2
LANES = 128
F32, BF16, I32 = jnp.float32, jnp.bfloat16, jnp.int32


def matmul(a, b, contract=((1,), (0,))):
    return lax.dot_general(a, b, (contract, ((), ())), preferred_element_type=F32)


def placement(ids_t, per_group, slots):
    n_tok = ids_t.shape[1]
    slot = lax.broadcasted_iota(I32, (GROUPS * slots, n_tok), 0)
    member = ids_t[0:1, :] // per_group == slot // slots
    earlier = (
        lax.broadcasted_iota(I32, (n_tok, n_tok), 0) < lax.broadcasted_iota(I32, (n_tok, n_tok), 1)
    )
    place = matmul(member.astype(F32).astype(BF16), earlier.astype(F32).astype(BF16))
    return (member & (place.astype(I32) == slot % slots)).astype(F32).astype(BF16)


def each(first, last, action):
    def go(k, carry):
        action(k)
        return carry
    lax.fori_loop(first, last, go, 0)


def kernel(
    nf, nt,
    tokens, ids_t, weights_t, gain, gate, up, down,
    gate_out, up_out, down_out, ret,
    wf, ws, xs, vs, xr, vr, wc, hs, ps, pr, qs, qr, rs,
    load_sem, wsend, wrecv, xsend, xrecv, vsend, vrecv, msend, mrecv, nsend, nrecv, gsend, grecv,
    psend, precv, qsend, qrecv, rsend, rrecv,
):
    f, t = lax.axis_index("fs"), lax.axis_index("tp")
    experts, rows, hidden = gate.shape
    n_tok, d_model = tokens.shape
    per = experts // nf
    cols = d_model // nt
    width = nf // GROUPS
    slots = xs.shape[1]
    per_group = experts // GROUPS
    plane = width * slots
    parts = max(1, rows // LANES)
    part = rows // parts
    joint = max(1, LANES // rows)
    pieces = d_model // LANES
    per_owner = cols // LANES
    g, m = f // width, lax.rem(f, width)
    served = (gate_out, up_out, down_out)

    def target(k):
        return lax.rem(f + k, nf)

    def source(k):
        return lax.rem(f - k + nf, nf)

    def other(k):
        return lax.rem(t + k, nt)

    def mate(k):
        return lax.rem(m + k, width)

    def group(k):
        return lax.rem(g + k, GROUPS)

    def span(start, size):
        return pl.ds(pl.multiple_of(start * size, size), size)

    def loads(a, k):
        p = target(k)
        return pltpu.make_async_copy(
            (gate, up, down)[a].at[pl.ds(p * per, per)],
            wf.at[a % 2, pl.ds(p * per, per)],
            load_sem.at[a, k],
        )

    def remote(src, dst, send, recv, device):
        return pltpu.make_async_remote_copy(
            src_ref=src, dst_ref=dst, send_sem=send, recv_sem=recv,
            device_id=device, device_id_type=MESH,
        )

    def weight_copy(a, p, src):
        return remote(
            ws.at[a, pl.ds(p * per, per)],
            served[a].at[:, span(src, rows), :],
            wsend.at[a, 0, p], wrecv.at[a, 0, src], {"fs": p},
        )

    def down_copy(h, p, src):
        return remote(
            ws.at[2, pl.ds(p * per, per), span(h, part), :],
            down_out.at[:, span(src * parts + h, part), :],
            wsend.at[2, h, p], wrecv.at[2, h, src], {"fs": p},
        )

    def token_copy(to, src):
        return remote(
            xs.at[to], xr.at[t, src, m], xsend.at[to], xrecv.at[src], {"fs": to * width + m}
        )

    def share_copy(to, src):
        return remote(vs.at[to], vr.at[src, m], vsend.at[to], vrecv.at[src], {"fs": to * width + m})

    def token_relay(to, src):
        return remote(
            xr.at[t, :, src], xr.at[t, :, src], msend.at[to], mrecv.at[src], {"fs": g * width + to}
        )

    def share_relay(to, src):
        return remote(
            vr.at[:, src], vr.at[:, src], nsend.at[to], nrecv.at[src], {"fs": g * width + to}
        )

    def gather_copy(to, src):
        return remote(xr.at[src], xr.at[src], gsend.at[to], grecv.at[src], {"tp": to})

    def partial_copy(c, to, src):
        return remote(
            ps.at[c, span(to, plane), :], pr.at[src, c],
            psend.at[c, to], precv.at[c, src], {"tp": to},
        )

    def mate_copy(c, to, src):
        return remote(
            qs.at[c, to], qr.at[src, c], qsend.at[c, to], qrecv.at[c, src], {"fs": g * width + to}
        )

    def return_copy(c, to_fs, to_tp, src):
        i = lax.rem(c, per_owner)
        return remote(
            rs.at[c], ret.at[i, span(src, slots), :],
            rsend.at[c], rrecv.at[src, i], {"fs": to_fs, "tp": to_tp},
        )

    each(1, nf, lambda k: loads(0, k).start())
    loads(0, 0).start()

    barrier = pltpu.get_barrier_semaphore()
    each(1, nf, lambda k: pl.semaphore_signal(
        barrier, inc=1, device_id={"fs": target(k)}, device_id_type=MESH))
    each(1, nt, lambda k: pl.semaphore_signal(
        barrier, inc=1, device_id={"tp": other(k)}, device_id_type=MESH))
    pl.semaphore_wait(barrier, nf + nt - 2)

    square = lax.broadcasted_iota(I32, (rows, rows), 0) == lax.broadcasted_iota(I32, (rows, rows), 1)
    gain_column = jnp.sum(jnp.where(square, gain[...], 0.0), axis=1, keepdims=True)

    def converted(a, n):
        value = wf[a % 2, n]
        if a < 2:
            value = value * gain_column
        return value.astype(BF16)

    def send_weights(a):
        def load_next(k):
            if a < 2:
                loads(a + 1, k).start()

        def one(k):
            p = target(k)
            loads(a, k).wait()
            load_next(k)
            for e in range(per):
                ws[a, p * per + e] = converted(a, p * per + e)
            if a < 2:
                weight_copy(a, p, f).start()
            else:
                down_copy(0, p, f).start()
        each(1, nf, one)
        loads(a, 0).wait()
        load_next(0)
        for e in range(per):
            served[a][e, span(f, rows), :] = converted(a, f * per + e)
        if a == 2:
            for h in range(1, parts):
                each(1, nf, lambda k: down_copy(h, target(k), f).start())

    send_weights(0)

    wide = tokens[...].astype(F32)
    scale = lax.rsqrt(jnp.mean(wide * wide, axis=1, keepdims=True) + EPSILON)
    own = tokens[:, span(t, cols)].astype(F32)
    normed = (own * scale).astype(BF16)
    chosen = placement(ids_t, per_group, slots)
    xs[...] = matmul(chosen, normed).reshape(GROUPS, slots, cols).astype(BF16)
    vs[...] = jnp.zeros(vs.shape, F32)
    row = lax.broadcasted_iota(I32, (vs.shape[1], n_tok), 0)
    for i in range(GROUPS):
        value = jnp.zeros((vs.shape[1], n_tok), F32)
        for r in range(ids_t.shape[0]):
            value += jnp.where(
                (row < per_group) & (row + i * per_group == ids_t[r:r + 1, :]),
                weights_t[r:r + 1, :], 0.0)
        high = value.astype(BF16)
        low = (value - high.astype(F32)).astype(BF16)
        here = chosen[i * slots:(i + 1) * slots]
        vs[i, :, 0:slots] = (
            matmul(high, here, ((1,), (1,))) + matmul(low, here, ((1,), (1,))))

    def dispatch(k):
        token_copy(group(k), g).start()
        share_copy(group(k), g).start()
    each(1, GROUPS, dispatch)
    xr[t, g, m] = xs[g]
    vr[g, m] = vs[g]

    send_weights(1)
    send_weights(2)

    def arrive(k):
        token_copy(g, group(k)).wait_recv()
        share_copy(g, group(k)).wait_recv()
    each(1, GROUPS, arrive)

    def relay(k):
        token_relay(mate(k), m).start()
        share_relay(mate(k), m).start()
    each(1, width, relay)

    def relayed(k):
        token_relay(m, mate(k)).wait_recv()
        share_relay(m, mate(k)).wait_recv()
    each(1, width, relayed)
    each(1, nt, lambda k: gather_copy(other(k), t).start())

    eye = lax.broadcasted_iota(I32, (slots, n_tok), 0) == lax.broadcasted_iota(I32, (slots, n_tok), 1)

    def shares(n):
        i, w = n // width, lax.rem(n, width)
        for e in range(per):
            line = vr[i, w, pl.ds(m * per + e, 1), :]
            column = jnp.sum(jnp.where(eye, line, 0.0), axis=1, keepdims=True)
            wc[e, span(n, slots), :] = jnp.broadcast_to(column, (slots, LANES))
    each(0, nf, shares)

    each(1, nt, lambda k: gather_copy(t, other(k)).wait_recv())

    def product(a, e, i):
        total = jnp.zeros((plane, hidden), F32)
        for o in range(nt):
            left = xr[o, i].reshape(plane, cols)
            total += matmul(left, served[a][e, o * cols:(o + 1) * cols, :])
        return total * d_model ** (-0.5)

    each(1, nf, lambda k: weight_copy(0, f, source(k)).wait_recv())
    each(1, nf, lambda k: weight_copy(1, f, source(k)).wait_recv())

    def activate(i):
        for e in range(per):
            v = product(0, e, i)
            value = v / (1.0 + jnp.exp(-v)) * product(1, e, i)
            value = value * wc[e, span(i, plane), 0:1]
            hs[span(i, plane), e * hidden:(e + 1) * hidden] = value.astype(BF16)
    each(0, GROUPS, activate)

    hidden_scale = (hidden * nt) ** (-0.5)
    blocks = pieces // parts
    first_block = g * width // joint

    def piece_at(n):
        return (first_block ^ lax.rem(n, blocks)) * parts + n // blocks

    def multiply(n):
        c = piece_at(n)
        h = lax.rem(c, parts)
        for q in range(joint):
            s = c // parts * joint + q

            @pl.when(s != f)
            def _():
                down_copy(h, f, s).wait_recv()
        value = jnp.zeros((nf * slots, LANES), F32)
        for e in range(per):
            value += matmul(
                hs[:, e * hidden:(e + 1) * hidden], down_out[e, span(c, LANES), :], ((1,), (1,)))
        ps[c] = (value * hidden_scale).astype(BF16)
        each(1, nt, lambda k: partial_copy(c, other(k), t).start())

    def reduce(n):
        c = piece_at(n)
        each(1, nt, lambda k: partial_copy(c, t, other(k)).wait_recv())
        total = ps[c, span(t, plane), :].astype(F32)
        for k in range(1, nt):
            total += pr[other(k), c].astype(F32)
        qs[c] = total.astype(BF16).reshape(width, slots, LANES)
        each(1, width, lambda k: mate_copy(c, mate(k), m).start())

    def give_back(n):
        c = piece_at(n)
        each(1, width, lambda k: mate_copy(c, m, mate(k)).wait_recv())
        total = qs[c, m].astype(F32)
        for k in range(1, width):
            total += qr[mate(k), c].astype(F32)
        rs[c] = total.astype(BF16)
        owner = c // per_owner
        local = (t == g) & (owner == t)

        @pl.when(local)
        def _():
            ret[lax.rem(c, per_owner), span(g, slots), :] = rs[c]

        @pl.when(jnp.logical_not(local))
        def _():
            return_copy(c, t * width + m, owner, g).start()

    def step(n):
        @pl.when(n < pieces)
        def _():
            multiply(n)

        @pl.when((n >= LAG) & (n < pieces + LAG))
        def _():
            reduce(n - LAG)

        @pl.when(n >= 2 * LAG)
        def _():
            give_back(n - 2 * LAG)
    each(0, pieces + 2 * LAG, step)

    def returned(n):
        i, src = lax.rem(n, per_owner), n // per_owner

        @pl.when(jnp.logical_not((src == g) & (t == g)))
        def _():
            return_copy(t * per_owner + i, f, t, src).wait_recv()
    each(0, GROUPS * per_owner, returned)

    def drain(k):
        p = target(k)
        for a in range(2):
            weight_copy(a, p, f).wait_send()
        for h in range(parts):
            down_copy(h, p, f).wait_send()
    each(1, nf, drain)

    def drain_tokens(k):
        token_copy(group(k), g).wait_send()
        share_copy(group(k), g).wait_send()
    each(1, GROUPS, drain_tokens)

    def drain_relay(k):
        token_relay(mate(k), m).wait_send()
        share_relay(mate(k), m).wait_send()
    each(1, width, drain_relay)
    each(1, nt, lambda k: gather_copy(other(k), t).wait_send())

    def drain_piece(c):
        each(1, nt, lambda k: partial_copy(c, other(k), t).wait_send())
        each(1, width, lambda k: mate_copy(c, mate(k), m).wait_send())
        owner = c // per_owner

        @pl.when(jnp.logical_not((t == g) & (owner == t)))
        def _():
            return_copy(c, t * width + m, owner, g).wait_send()
    each(0, pieces, drain_piece)


def finish_kernel(ids_t, ret, gate, up, down, gate_out, up_out, down_out, combined, sem, *, per_group):
    outs = [
        pltpu.make_async_copy(source, target, sem.at[a])
        for a, (source, target) in enumerate(((gate, gate_out), (up, up_out), (down, down_out)))
    ]
    for copy in outs:
        copy.start()
    chunks, slots, width = ret.shape
    chosen = placement(ids_t, per_group, slots // GROUPS)
    for i in range(chunks):
        value = matmul(chosen, ret[i], ((0,), (0,)))
        combined[:, i * width:(i + 1) * width] = value.astype(BF16)
    for copy in outs:
        copy.wait()


def body(nf, nt, tokens, route_ids, route_weights, norm_gain, gate_weight, up_weight, down_weight):
    experts, rows, hidden = gate_weight.shape
    n_tok, d_model = tokens.shape
    per = experts // nf
    cols = d_model // nt
    slots = n_tok // route_ids.shape[1]
    width = nf // GROUPS
    per_group = experts // GROUPS
    lines = max(8, per_group)
    parts = max(1, rows // LANES)
    pieces = d_model // LANES
    per_owner = cols // LANES
    shape = (per, nf * rows, hidden)
    vmem, anywhere = pl.BlockSpec(memory_space=pltpu.VMEM), pl.BlockSpec(memory_space=pl.ANY)
    dma = pltpu.SemaphoreType.DMA
    ids_t, weights_t = route_ids.T, route_weights.T
    *served, ret = pl.pallas_call(
        functools.partial(kernel, nf, nt),
        out_shape=[pltpu.VMEM(shape, BF16)] * 3
        + [pltpu.VMEM((per_owner, GROUPS * slots, LANES), BF16)],
        in_specs=[vmem] * 4 + [anywhere] * 3,
        out_specs=[vmem] * 4,
        scratch_shapes=[
            pltpu.VMEM((2, experts, rows, hidden), F32),
            pltpu.VMEM((3, experts, rows, hidden), BF16),
            pltpu.VMEM((GROUPS, slots, cols), BF16),
            pltpu.VMEM((GROUPS, lines, n_tok), F32),
            pltpu.VMEM((nt, GROUPS, width, slots, cols), BF16),
            pltpu.VMEM((GROUPS, width, lines, n_tok), F32),
            pltpu.VMEM((per, nf * slots, LANES), F32),
            pltpu.VMEM((nf * slots, per * hidden), BF16),
            pltpu.VMEM((pieces, nf * slots, LANES), BF16),
            pltpu.VMEM((nt, pieces, width * slots, LANES), BF16),
            pltpu.VMEM((pieces, width, slots, LANES), BF16),
            pltpu.VMEM((width, pieces, slots, LANES), BF16),
            pltpu.VMEM((pieces, slots, LANES), BF16),
            dma((3, nf)),
            dma((3, parts, nf)), dma((3, parts, nf)),
            dma((GROUPS,)), dma((GROUPS,)),
            dma((GROUPS,)), dma((GROUPS,)),
            dma((width,)), dma((width,)),
            dma((width,)), dma((width,)),
            dma((nt,)), dma((nt,)),
            dma((pieces, nt)), dma((pieces, nt)),
            dma((pieces, width)), dma((pieces, width)),
            dma((pieces,)), dma((GROUPS, per_owner)),
        ],
        compiler_params=pltpu.CompilerParams(
            collective_id=0, has_side_effects=True, vmem_limit_bytes=54 * 1024 * 1024
        ),
    )(tokens, ids_t, weights_t, norm_gain[None, :], gate_weight, up_weight, down_weight)
    out = jax.ShapeDtypeStruct(shape, BF16)
    return pl.pallas_call(
        functools.partial(finish_kernel, per_group=per_group),
        out_shape=(out, out, out, jax.ShapeDtypeStruct((n_tok, cols), BF16)),
        in_specs=[vmem] * 5,
        out_specs=(anywhere, anywhere, anywhere, vmem),
        scratch_shapes=[dma((3,))],
        compiler_params=pltpu.CompilerParams(vmem_limit_bytes=16 * 1024 * 1024),
    )(ids_t, ret, *served)


def solution(mesh):
    split = P(None, "fs", "tp")
    served = P("fs", None, "tp")
    return jax.shard_map(
        functools.partial(body, mesh.shape["fs"], mesh.shape["tp"]),
        mesh=mesh,
        in_specs=(P("fs", None), P("fs", None), P("fs", None), P("fs"), split, split, split),
        out_specs=(served, served, served, P("fs", "tp")),
        check_vma=False,
    )
```

time: 182 us -> 178 us (0.978)
  the two profiles are of different devices: /device:TPU:0 before, /device:TPU:1 now
where the time goes in v1:
time: 178 us; the launch traced here: 175 us
  Pallas kernels  174 us (98%)
    pallas_call x1, Pallas kernels, body(): pl.pallas_call(functools.partial(kernel, nf, nt), out_shape=[pltpu.VMEM(s...  171 us

profile of v1, /device:TPU:1, one launch (start us, length us, event | category | flops | bytes accessed | tf_op | source)
XLA Modules:
  0.0 174.8 jit_solution(9640877246472448581)
XLA Ops:
  0.6 0.0 copy-start
  0.6 170.8 %shard_map.102 = (bf16[2,2048,256]{2,1,0:T(8,128)(2,1)S(1)}, bf16[2,2048,256]{2,1,0:T(8,128)(2,1)S(1)}, bf16[2,2048,256]{2,1,0:T(8,128)(2,1)S(1)}, bf16[4,256,128]{2,1,0:T(8,128)(2,1)S(1)}) custom-call(bf16[128,2048]{1,0:T(8,128)(2,1)} %tokens.1, s32[2,128]{1,0:T(2,128)} %bitcast.3, f32[2,128]{1,0:T(2,128)} %bitcast.5, f32[1,256]{1,0:T(1,128)} %bitcast.6, ...), custom_call_target="tpu_custom_call" | custom-call | tf_op jit(solution)/shard_map/pallas_call | solution.py:405
  171.4 0.0 copy-done
  171.4 3.4 %shard_map.103 = (bf16[2,2048,256]{2,1,0:T(8,128)(2,1)}, bf16[2,2048,256]{2,1,0:T(8,128)(2,1)}, bf16[2,2048,256]{2,1,0:T(8,128)(2,1)}, bf16[128,512]{1,0:T(8,128)(2,1)}) custom-call(s32[2,128]{1,0:T(2,128)S(1)} %bitcast.4, bf16[4,256,128]{2,1,0:T(8,128)(2,1)S(1)} %get-tuple-element.8.ret, bf16[2,2048,256]{2,1,0:T(8,128)(2,1)S(1)} %get-tuple-element.9.gate, ...), custom_call_target="tpu_custom_call" | custom-call | tf_op jit(solution)/shard_map/pallas_call | solution.py:441
Async XLA Ops:
  0.6 170.8 %copy-start = (s32[128,2]{0,1:T(2,128)S(1)}, s32[128,2]{0,1:T(2,128)}, u32[]{:S(2)}) copy-start(s32[128,2]{0,1:T(2,128)} %param.8) | copy-start | bytes 3076

commit v2 on v1

v2 whole, which is shorter than its diff:
```python
import functools

import jax
import jax.numpy as jnp
from jax import lax
from jax.experimental import pallas as pl
from jax.experimental.pallas import tpu as pltpu
from jax.sharding import PartitionSpec as P

GROUPS = 4
EPSILON = 1e-06
MESH = pl.DeviceIdType.MESH
PAIR_LAG, CREW_LAG = 1, 3
LANES = 128
F32, BF16, I32 = jnp.float32, jnp.bfloat16, jnp.int32


def matmul(a, b, contract=((1,), (0,))):
    return lax.dot_general(a, b, (contract, ((), ())), preferred_element_type=F32)


def placement(ids_t, per_group, slots):
    n_tok = ids_t.shape[1]
    slot = lax.broadcasted_iota(I32, (GROUPS * slots, n_tok), 0)
    member = ids_t[0:1, :] // per_group == slot // slots
    earlier = (
        lax.broadcasted_iota(I32, (n_tok, n_tok), 0) < lax.broadcasted_iota(I32, (n_tok, n_tok), 1)
    )
    place = matmul(member.astype(F32).astype(BF16), earlier.astype(F32).astype(BF16))
    return (member & (place.astype(I32) == slot % slots)).astype(F32).astype(BF16)


def each(first, last, action):
    def go(k, carry):
        action(k)
        return carry
    lax.fori_loop(first, last, go, 0)


def kernel(
    nf, nt,
    tokens, ids_t, weights_t, gain, gate, up, down,
    gate_out, up_out, down_out, ret,
    wf, ws, xs, vs, xr, vr, wc, hs, ps, pr, qs, qr, rs,
    load_sem, wsend, wrecv, drecv, xsem, vsem, msem, nsem, gsem, psend, precv, qsend, qrecv, rsem,
):
    f, t = lax.axis_index("fs"), lax.axis_index("tp")
    experts, rows, hidden = gate.shape
    n_tok, d_model = tokens.shape
    per = experts // nf
    cols = d_model // nt
    width = nf // GROUPS
    slots = n_tok // ids_t.shape[0]
    split = nt // GROUPS
    share = slots // split
    per_group = experts // GROUPS
    plane = width * share
    parts = max(1, rows // LANES)
    part = rows // parts
    joint = max(1, LANES // rows)
    pieces = d_model // LANES
    per_owner = cols // LANES
    g, m = f // width, lax.rem(f, width)
    shift = t // 2 + nt // 2 * lax.rem(t, 2)
    home, rest = shift // split, lax.rem(shift, split)
    crews = nt // 2 * width
    served = (gate_out, up_out, down_out)

    def target(k):
        return lax.rem(jnp.where(f < nf // 2, f + k, f + nf - k), nf)

    def other(k):
        return lax.rem(t + k, nt)

    def mate(k):
        return lax.rem(m + k, width)

    def group(k):
        return lax.rem(g + k, GROUPS)

    def span(start, size):
        return pl.ds(pl.multiple_of(start * size, size), size)

    def loads(a, k):
        p = target(k)
        return pltpu.make_async_copy(
            (gate, up, down)[a].at[pl.ds(p * per, per)],
            wf.at[a % 2, pl.ds(p * per, per)],
            load_sem.at[k],
        )

    def remote(src, dst, send, recv, device):
        return pltpu.make_async_remote_copy(
            src_ref=src, dst_ref=dst, send_sem=send, recv_sem=recv,
            device_id=device, device_id_type=MESH,
        )

    def settle(ref, sem):
        pltpu.make_async_copy(ref, ref, sem).wait()

    def weight_copy(a, p, src):
        return remote(
            ws.at[a, pl.ds(p * per, per)],
            served[a].at[:, span(src, rows), :],
            wsend.at[a], wrecv.at[a], {"fs": p},
        )

    def down_copy(h, p, src):
        return remote(
            ws.at[2, pl.ds(p * per, per), span(h, part), :],
            down_out.at[:, span(src * parts + h, part), :],
            wsend.at[2], drecv.at[h, src], {"fs": p},
        )

    def token_copy(to, src):
        return remote(
            xs.at[to], xr.at[t, pl.ds(src * split, split), m], xsem.at[0], xsem.at[1], {"fs": to * width + m}
        )

    def share_copy(to, src):
        return remote(vs.at[to], vr.at[src, m], vsem.at[0], vsem.at[1], {"fs": to * width + m})

    def token_relay(to, src):
        return remote(
            xr.at[t, :, src], xr.at[t, :, src], msem.at[0], msem.at[1], {"fs": g * width + to}
        )

    def share_relay(to, src):
        return remote(
            vr.at[:, src], vr.at[:, src], nsem.at[0], nsem.at[1], {"fs": g * width + to}
        )

    def gather_copy(to, src):
        return remote(xr.at[src], xr.at[src], gsem.at[0], gsem.at[1], {"tp": to})

    def partial_copy(c, to):
        return remote(
            ps.at[c, lax.rem(to, 2)], pr.at[c], psend, precv.at[c], {"tp": t // 2 * 2 + lax.rem(to, 2)}
        )

    def crew(k):
        return lax.rem(t // 2 * width + m + k, crews)

    def crew_copy(c, to, src):
        return remote(
            qs.at[c, to], qr.at[src, c], qsend, qrecv.at[c],
            {"fs": g * width + lax.rem(to, width), "tp": to // width * 2 + lax.rem(t, 2)},
        )

    def return_copy(c, to_fs, to_tp, src):
        i = lax.rem(c, per_owner)
        return remote(
            rs.at[c], ret.at[i, span(src, share), :],
            rsem.at[0], rsem.at[1], {"fs": to_fs, "tp": to_tp},
        )

    each(1, nf, lambda k: loads(0, k).start())
    loads(0, 0).start()

    barrier = pltpu.get_barrier_semaphore()
    each(1, nf, lambda k: pl.semaphore_signal(
        barrier, inc=1, device_id={"fs": target(k)}, device_id_type=MESH))
    each(1, nt, lambda k: pl.semaphore_signal(
        barrier, inc=1, device_id={"tp": other(k)}, device_id_type=MESH))
    wide = tokens[...].astype(F32)
    scale = lax.rsqrt(jnp.mean(wide * wide, axis=1, keepdims=True) + EPSILON)
    own = tokens[:, span(t, cols)].astype(F32)
    normed = (own * scale).astype(BF16)
    chosen = placement(ids_t, per_group, slots)
    xs[...] = matmul(chosen, normed).reshape(GROUPS, split, share, cols).astype(BF16)
    vs[...] = jnp.zeros(vs.shape, F32)
    row = lax.broadcasted_iota(I32, (vs.shape[1], n_tok), 0)
    for i in range(GROUPS):
        value = jnp.zeros((vs.shape[1], n_tok), F32)
        for r in range(ids_t.shape[0]):
            value += jnp.where(
                (row < per_group) & (row + i * per_group == ids_t[r:r + 1, :]),
                weights_t[r:r + 1, :], 0.0)
        high = value.astype(BF16)
        low = (value - high.astype(F32)).astype(BF16)
        here = chosen[i * slots:(i + 1) * slots]
        vs[i, :, 0:slots] = (
            matmul(high, here, ((1,), (1,))) + matmul(low, here, ((1,), (1,))))

    with jax.named_scope('barrier'):
        pl.semaphore_wait(barrier, nf + nt - 2)

    def dispatch(k):
        token_copy(group(k), g).start()
        share_copy(group(k), g).start()
    each(1, GROUPS, dispatch)
    for q in range(split):
        xr[t, g * split + q, m] = xs[g, q]
    vr[g, m] = vs[g]

    square = lax.broadcasted_iota(I32, (rows, rows), 0) == lax.broadcasted_iota(I32, (rows, rows), 1)
    gain_column = jnp.sum(jnp.where(square, gain[...], 0.0), axis=1, keepdims=True)

    def converted(a, n):
        value = wf[a % 2, n]
        if a < 2:
            value = value * gain_column
        return value.astype(BF16)

    def send_weights(a):
        def load_next(k):
            if a < 2:
                loads(a + 1, k).start()

        def one(k):
            p = target(k)
            loads(a, k).wait()
            load_next(k)
            for e in range(per):
                ws[a, p * per + e] = converted(a, p * per + e)
            if a < 2:
                weight_copy(a, p, f).start()
        each(1, nf, one)
        loads(a, 0).wait()
        load_next(0)
        for e in range(per):
            served[a][e, span(f, rows), :] = converted(a, f * per + e)

    def send_down():
        for h in range(parts):
            each(1, nf, lambda k: down_copy(h, target(k), f).start())

    with jax.named_scope('send0'):
        send_weights(0)

    with jax.named_scope('send1'):
        send_weights(1)
    with jax.named_scope('send2'):
        send_weights(2)
    outer = (g == 0) | (g == GROUPS - 1)
    pl.when(jnp.logical_not(outer))(send_down)

    with jax.named_scope('arrive'):
        settle(xs.at[0:GROUPS - 1], xsem.at[1])
        settle(vs.at[0:GROUPS - 1], vsem.at[1])

    def relay(k):
        token_relay(mate(k), m).start()
        share_relay(mate(k), m).start()
    each(1, width, relay)

    with jax.named_scope('relayed'):
        settle(xr.at[t, :, 0:width - 1], msem.at[1])
        settle(vr.at[:, 0:width - 1], nsem.at[1])
    each(1, nt, lambda k: gather_copy(other(k), t).start())

    lane = lax.broadcasted_iota(I32, (share, n_tok), 1) - lax.broadcasted_iota(I32, (share, n_tok), 0)

    def shares(n):
        i, w = n // width, lax.rem(n, width)
        eye = lane == lax.rem(i, split) * share
        for e in range(per):
            line = vr[i // split, w, pl.ds(m * per + e, 1), :]
            column = jnp.sum(jnp.where(eye, line, 0.0), axis=1, keepdims=True)
            wc[e, span(n, share), :] = jnp.broadcast_to(column, (share, LANES))
    each(0, nt * width, shares)

    with jax.named_scope('gather'):
        settle(xr.at[0:nt - 1], gsem.at[1])

    def product(a, e, i):
        total = jnp.zeros((plane, hidden), F32)
        for o in range(nt):
            left = xr[o, i].reshape(plane, cols)
            total += matmul(left, served[a][e, o * cols:(o + 1) * cols, :])
        return total * d_model ** (-0.5)

    with jax.named_scope('wait_gate'):
        settle(ws.at[0, 0:experts - per], wrecv.at[0])
    with jax.named_scope('wait_up'):
        settle(ws.at[1, 0:experts - per], wrecv.at[1])

    def activate(i):
        for e in range(per):
            v = product(0, e, i)
            value = v / (1.0 + jnp.exp(-v)) * product(1, e, i)
            value = value * wc[e, span(i, plane), 0:1]
            hs[span(i, plane), e * hidden:(e + 1) * hidden] = value.astype(BF16)
    pl.when(outer)(send_down)
    with jax.named_scope('activate'):
        each(0, nt, activate)

    hidden_scale = (hidden * nt) ** (-0.5)
    blocks = pieces // parts
    quarter = pieces // GROUPS
    wide_blocks = blocks // GROUPS
    low = g < GROUPS // 2

    def piece_at(n):
        i, r = n // quarter, lax.rem(n, quarter)
        far = jnp.where(low, GROUPS + 1 - i, i - 2)
        z = jnp.where(i < 2, g ^ i, far)
        return (z * wide_blocks + lax.rem(r, wide_blocks)) * parts + r // wide_blocks

    def multiply(n):
        c = piece_at(n)
        h = lax.rem(c, parts)
        for q in range(joint):
            s = c // parts * joint + q

            @pl.when(s != f)
            def _():
                with jax.named_scope('wait_piece'):
                    down_copy(h, f, s).wait_recv()
        value = jnp.zeros((nt * plane, LANES), F32)
        for e in range(per):
            value += matmul(
                hs[:, e * hidden:(e + 1) * hidden], down_out[e, span(c, LANES), :], ((1,), (1,)))
        ps[c] = (value * hidden_scale).astype(BF16).reshape(2, nt // 2, plane, LANES)
        partial_copy(c, t + 1).start()

    def reduce(n):
        c = piece_at(n)
        with jax.named_scope('wait_partial'):
            partial_copy(c, t).wait_recv()
        total = ps[c, lax.rem(t, 2)].astype(F32) + pr[c].astype(F32)
        qs[c] = total.astype(BF16).reshape(crews, share, LANES)
        each(1, crews, lambda k: crew_copy(c, crew(k), crew(0)).start())

    def give_back(n):
        c = piece_at(n)
        with jax.named_scope('wait_mate'):
            settle(qs.at[c, 0:crews - 1], qrecv.at[c])
        total = qs[c, crew(0)].astype(F32)
        for k in range(1, crews):
            total += qr[crew(k), c].astype(F32)
        rs[c] = total.astype(BF16)
        owner = c // per_owner
        local = (home == g) & (owner == t)

        @pl.when(local)
        def _():
            ret[lax.rem(c, per_owner), span(g * split + rest, share), :] = rs[c]

        @pl.when(jnp.logical_not(local))
        def _():
            return_copy(c, home * width + m, owner, g * split + rest).start()

    def step(n):
        @pl.when(n < pieces)
        def _():
            multiply(n)

        @pl.when((n >= PAIR_LAG) & (n < pieces + PAIR_LAG))
        def _():
            reduce(n - PAIR_LAG)

        @pl.when(n >= CREW_LAG)
        def _():
            give_back(n - CREW_LAG)
    each(0, pieces + CREW_LAG, step)

    own_share = pieces - per_owner

    @pl.when(home == g)
    def _():
        settle(ret.at[:, 0:GROUPS * slots - share], rsem.at[1])
        settle(rs.at[0:own_share], rsem.at[0])

    @pl.when(home != g)
    def _():
        settle(ret, rsem.at[1])
        settle(rs, rsem.at[0])

    for a in range(3):
        settle(ws.at[a, 0:experts - per], wsend.at[a])
    settle(xs.at[0:GROUPS - 1], xsem.at[0])
    settle(vs.at[0:GROUPS - 1], vsem.at[0])
    settle(xr.at[t, :, 0:width - 1], msem.at[0])
    settle(vr.at[:, 0:width - 1], nsem.at[0])
    settle(xr.at[0:nt - 1], gsem.at[0])
    settle(pr, psend)
    settle(qs.at[:, 0:crews - 1], qsend)


def finish_kernel(ids_t, ret, gate, up, down, gate_out, up_out, down_out, combined, sem, *, per_group):
    outs = [
        pltpu.make_async_copy(source, target, sem.at[a])
        for a, (source, target) in enumerate(((gate, gate_out), (up, up_out), (down, down_out)))
    ]
    for copy in outs:
        copy.start()
    chunks, slots, width = ret.shape
    chosen = placement(ids_t, per_group, slots // GROUPS)
    for i in range(chunks):
        value = matmul(chosen, ret[i], ((0,), (0,)))
        combined[:, i * width:(i + 1) * width] = value.astype(BF16)
    for copy in outs:
        copy.wait()


def body(nf, nt, tokens, route_ids, route_weights, norm_gain, gate_weight, up_weight, down_weight):
    experts, rows, hidden = gate_weight.shape
    n_tok, d_model = tokens.shape
    per = experts // nf
    cols = d_model // nt
    slots = n_tok // route_ids.shape[1]
    width = nf // GROUPS
    per_group = experts // GROUPS
    lines = max(8, per_group)
    crews = nt // 2 * width
    split = nt // GROUPS
    share = slots // split
    parts = max(1, rows // LANES)
    pieces = d_model // LANES
    per_owner = cols // LANES
    shape = (per, nf * rows, hidden)
    vmem, anywhere = pl.BlockSpec(memory_space=pltpu.VMEM), pl.BlockSpec(memory_space=pl.ANY)
    dma = pltpu.SemaphoreType.DMA
    ids_t, weights_t = route_ids.T, route_weights.T
    *served, ret = pl.pallas_call(
        functools.partial(kernel, nf, nt),
        out_shape=[pltpu.VMEM(shape, BF16)] * 3
        + [pltpu.VMEM((per_owner, GROUPS * slots, LANES), BF16)],
        in_specs=[vmem] * 4 + [anywhere] * 3,
        out_specs=[vmem] * 4,
        scratch_shapes=[
            pltpu.VMEM((2, experts, rows, hidden), F32),
            pltpu.VMEM((3, experts, rows, hidden), BF16),
            pltpu.VMEM((GROUPS, split, share, cols), BF16),
            pltpu.VMEM((GROUPS, lines, n_tok), F32),
            pltpu.VMEM((nt, nt, width, share, cols), BF16),
            pltpu.VMEM((GROUPS, width, lines, n_tok), F32),
            pltpu.VMEM((per, nf * slots, LANES), F32),
            pltpu.VMEM((nf * slots, per * hidden), BF16),
            pltpu.VMEM((pieces, 2, nt // 2, width * share, LANES), BF16),
            pltpu.VMEM((pieces, nt // 2, width * share, LANES), BF16),
            pltpu.VMEM((pieces, crews, share, LANES), BF16),
            pltpu.VMEM((crews, pieces, share, LANES), BF16),
            pltpu.VMEM((pieces, share, LANES), BF16),
            dma((nf,)), dma((3,)), dma((2,)), dma((parts, nf)),
            dma((2,)), dma((2,)), dma((2,)), dma((2,)), dma((2,)),
            dma, dma((pieces,)), dma, dma((pieces,)), dma((2,)),
        ],
        compiler_params=pltpu.CompilerParams(
            collective_id=0, has_side_effects=True, vmem_limit_bytes=54 * 1024 * 1024
        ),
    )(tokens, ids_t, weights_t, norm_gain[None, :], gate_weight, up_weight, down_weight)
    out = jax.ShapeDtypeStruct(shape, BF16)
    return pl.pallas_call(
        functools.partial(finish_kernel, per_group=per_group),
        out_shape=(out, out, out, jax.ShapeDtypeStruct((n_tok, cols), BF16)),
        in_specs=[vmem] * 5,
        out_specs=(anywhere, anywhere, anywhere, vmem),
        scratch_shapes=[dma((3,))],
        compiler_params=pltpu.CompilerParams(vmem_limit_bytes=16 * 1024 * 1024),
    )(ids_t, ret, *served)


def solution(mesh):
    split = P(None, "fs", "tp")
    served = P("fs", None, "tp")
    return jax.shard_map(
        functools.partial(body, mesh.shape["fs"], mesh.shape["tp"]),
        mesh=mesh,
        in_specs=(P("fs", None), P("fs", None), P("fs", None), P("fs"), split, split, split),
        out_specs=(served, served, served, P("fs", "tp")),
        check_vma=False,
    )
```

time: 178 us -> 166 us (0.933); the launches traced: 175 us -> 166 us
  Pallas kernels: 174 us -> 166 us
    pallas_call x1, Pallas kernels: 171 us -> 162 us  [body(): pl.pallas_call(functools.partial(kernel, nf, nt), out_shape=[pltpu.VMEM(s...]
where the time goes in v2:
time: 166 us
  Pallas kernels  166 us (100%)
    pallas_call x1, Pallas kernels, body(): pl.pallas_call(functools.partial(kernel, nf, nt), out_shape=[pltpu.VMEM(s...  162 us
    pallas_call x1, Pallas kernels, body(): pl.pallas_call(functools.partial(finish_kernel, per_group=per_group), out...  3.42 us

profile of v2, /device:TPU:1, one launch (start us, length us, event | category | flops | bytes accessed | tf_op | source)
XLA Modules:
  0.0 166.3 jit_solution(5052346673502086212)
XLA Ops:
  0.6 0.0 copy-start
  0.6 162.2 %shard_map.102 = (bf16[2,2048,256]{2,1,0:T(8,128)(2,1)S(1)}, bf16[2,2048,256]{2,1,0:T(8,128)(2,1)S(1)}, bf16[2,2048,256]{2,1,0:T(8,128)(2,1)S(1)}, bf16[4,256,128]{2,1,0:T(8,128)(2,1)S(1)}) custom-call(bf16[128,2048]{1,0:T(8,128)(2,1)} %tokens.1, s32[2,128]{1,0:T(2,128)} %bitcast.3, f32[2,128]{1,0:T(2,128)} %bitcast.5, f32[1,256]{1,0:T(1,128)} %bitcast.6, ...), custom_call_target="tpu_custom_call" | custom-call | tf_op jit(solution)/shard_map/pallas_call | solution.py:416
  162.8 0.0 copy-done
  162.8 3.4 %shard_map.103 = (bf16[2,2048,256]{2,1,0:T(8,128)(2,1)}, bf16[2,2048,256]{2,1,0:T(8,128)(2,1)}, bf16[2,2048,256]{2,1,0:T(8,128)(2,1)}, bf16[128,512]{1,0:T(8,128)(2,1)}) custom-call(s32[2,128]{1,0:T(2,128)S(1)} %bitcast.4, bf16[4,256,128]{2,1,0:T(8,128)(2,1)S(1)} %get-tuple-element.8.ret, bf16[2,2048,256]{2,1,0:T(8,128)(2,1)S(1)} %get-tuple-element.9.gate, ...), custom_call_target="tpu_custom_call" | custom-call | tf_op jit(solution)/shard_map/pallas_call | solution.py:445
Async XLA Ops:
  0.6 162.2 %copy-start = (s32[128,2]{0,1:T(2,128)S(1)}, s32[128,2]{0,1:T(2,128)}, u32[]{:S(2)}) copy-start(s32[128,2]{0,1:T(2,128)} %param.8) | copy-start | bytes 3076

commit v3 on v2

--- a/solution.py
+++ b/solution.py
@@ -39,10 +39,11 @@
 
 def kernel(
     nf, nt,
-    tokens, ids_t, weights_t, gain, gate, up, down,
+    tokens_in, ids_in, weights_in, gain_in, gate, up, down,
     gate_out, up_out, down_out, ret,
+    tokens, ids_t, weights_t, gain,
     wf, ws, xs, vs, xr, vr, wc, hs, ps, pr, qs, qr, rs,
-    load_sem, wsend, wrecv, drecv, xsem, vsem, msem, nsem, gsem, psend, precv, qsend, qrecv, rsem,
+    in_sem, load_sem, wsend, wrecv, drecv, xsem, vsem, msem, nsem, gsem, psend, precv, qsend, qrecv, rsem,
 ):
     f, t = lax.axis_index("fs"), lax.axis_index("tp")
     experts, rows, hidden = gate.shape
@@ -154,14 +155,22 @@
             rsem.at[0], rsem.at[1], {"fs": to_fs, "tp": to_tp},
         )
 
-    each(1, nf, lambda k: loads(0, k).start())
-    loads(0, 0).start()
-
     barrier = pltpu.get_barrier_semaphore()
     each(1, nf, lambda k: pl.semaphore_signal(
         barrier, inc=1, device_id={"fs": target(k)}, device_id_type=MESH))
     each(1, nt, lambda k: pl.semaphore_signal(
         barrier, inc=1, device_id={"tp": other(k)}, device_id_type=MESH))
+    inputs = [
+        pltpu.make_async_copy(src, dst, in_sem.at[i])
+        for i, (src, dst) in enumerate((
+            (tokens_in, tokens), (ids_in, ids_t), (weights_in, weights_t), (gain_in, gain)))
+    ]
+    for copy in inputs:
+        copy.start()
+    each(1, nf, lambda k: loads(0, k).start())
+    loads(0, 0).start()
+    for copy in inputs:
+        copy.wait()
     wide = tokens[...].astype(F32)
     scale = lax.rsqrt(jnp.mean(wide * wide, axis=1, keepdims=True) + EPSILON)
     own = tokens[:, span(t, cols)].astype(F32)
@@ -221,9 +230,10 @@
         for e in range(per):
             served[a][e, span(f, rows), :] = converted(a, f * per + e)
 
-    def send_down():
-        for h in range(parts):
-            each(1, nf, lambda k: down_copy(h, target(k), f).start())
+    def send_down(first, end):
+        for h in range(first, end):
+            last = nf if h == parts - 1 else 0
+            each(1, nf, lambda k: down_copy(h, target(last - k if last else k), f).start())
 
     with jax.named_scope('send0'):
         send_weights(0)
@@ -233,7 +243,7 @@
     with jax.named_scope('send2'):
         send_weights(2)
     outer = (g == 0) | (g == GROUPS - 1)
-    pl.when(jnp.logical_not(outer))(send_down)
+    pl.when(jnp.logical_not(outer))(lambda: send_down(0, parts))
 
     with jax.named_scope('arrive'):
         settle(xs.at[0:GROUPS - 1], xsem.at[1])
@@ -281,7 +291,7 @@
             value = v / (1.0 + jnp.exp(-v)) * product(1, e, i)
             value = value * wc[e, span(i, plane), 0:1]
             hs[span(i, plane), e * hidden:(e + 1) * hidden] = value.astype(BF16)
-    pl.when(outer)(send_down)
+    pl.when(outer)(lambda: send_down(0, parts))
     with jax.named_scope('activate'):
         each(0, nt, activate)
 
@@ -378,7 +388,9 @@
     settle(qs.at[:, 0:crews - 1], qsend)
 
 
-def finish_kernel(ids_t, ret, gate, up, down, gate_out, up_out, down_out, combined, sem, *, per_group):
+def finish_kernel(
+    ids_t, ret, gate, up, down, gate_out, up_out, down_out, combined, result, sem, *, per_group
+):
     outs = [
         pltpu.make_async_copy(source, target, sem.at[a])
         for a, (source, target) in enumerate(((gate, gate_out), (up, up_out), (down, down_out)))
@@ -389,9 +401,12 @@
     chosen = placement(ids_t, per_group, slots // GROUPS)
     for i in range(chunks):
         value = matmul(chosen, ret[i], ((0,), (0,)))
-        combined[:, i * width:(i + 1) * width] = value.astype(BF16)
+        result[:, i * width:(i + 1) * width] = value.astype(BF16)
+    last = pltpu.make_async_copy(result, combined, sem.at[3])
+    last.start()
     for copy in outs:
         copy.wait()
+    last.wait()
 
 
 def body(nf, nt, tokens, route_ids, route_weights, norm_gain, gate_weight, up_weight, down_weight):
@@ -417,9 +432,13 @@
         functools.partial(kernel, nf, nt),
         out_shape=[pltpu.VMEM(shape, BF16)] * 3
         + [pltpu.VMEM((per_owner, GROUPS * slots, LANES), BF16)],
-        in_specs=[vmem] * 4 + [anywhere] * 3,
+        in_specs=[anywhere] * 7,
         out_specs=[vmem] * 4,
         scratch_shapes=[
+            pltpu.VMEM((n_tok, d_model), BF16),
+            pltpu.VMEM(ids_t.shape, I32),
+            pltpu.VMEM(weights_t.shape, F32),
+            pltpu.VMEM((1, rows), F32),
             pltpu.VMEM((2, experts, rows, hidden), F32),
             pltpu.VMEM((3, experts, rows, hidden), BF16),
             pltpu.VMEM((GROUPS, split, share, cols), BF16),
@@ -433,7 +452,7 @@
             pltpu.VMEM((pieces, crews, share, LANES), BF16),
             pltpu.VMEM((crews, pieces, share, LANES), BF16),
             pltpu.VMEM((pieces, share, LANES), BF16),
-            dma((nf,)), dma((3,)), dma((2,)), dma((parts, nf)),
+            dma((4,)), dma((nf,)), dma((3,)), dma((2,)), dma((parts, nf)),
             dma((2,)), dma((2,)), dma((2,)), dma((2,)), dma((2,)),
             dma, dma((pieces,)), dma, dma((pieces,)), dma((2,)),
         ],
@@ -446,8 +465,8 @@
         functools.partial(finish_kernel, per_group=per_group),
         out_shape=(out, out, out, jax.ShapeDtypeStruct((n_tok, cols), BF16)),
         in_specs=[vmem] * 5,
-        out_specs=(anywhere, anywhere, anywhere, vmem),
-        scratch_shapes=[dma((3,))],
+        out_specs=(anywhere,) * 4,
+        scratch_shapes=[pltpu.VMEM((n_tok, cols), BF16), dma((4,))],
         compiler_params=pltpu.CompilerParams(vmem_limit_bytes=16 * 1024 * 1024),
     )(ids_t, ret, *served)
 

time: 166 us -> 164 us (0.988)
  Pallas kernels: 166 us -> 162 us
    pallas_call x1, Pallas kernels: 162 us -> 159 us  [body(): pl.pallas_call(functools.partial(kernel, nf, nt), out_shape=[pltpu.VMEM(s...]
where the time goes in v3:
time: 164 us; the launch traced here: 163 us
  Pallas kernels  162 us (99%)
    pallas_call x1, Pallas kernels, body(): pl.pallas_call(functools.partial(kernel, nf, nt), out_shape=[pltpu.VMEM(s...  159 us

profile of v3, /device:TPU:1, one launch (start us, length us, event | category | flops | bytes accessed | tf_op | source)
XLA Modules:
  0.0 162.9 jit_solution(9887026739857664526)
XLA Ops:
  0.6 0.0 copy-start
  0.6 159.5 %shard_map.102 = (bf16[2,2048,256]{2,1,0:T(8,128)(2,1)S(1)}, bf16[2,2048,256]{2,1,0:T(8,128)(2,1)S(1)}, bf16[2,2048,256]{2,1,0:T(8,128)(2,1)S(1)}, bf16[4,256,128]{2,1,0:T(8,128)(2,1)S(1)}) custom-call(bf16[128,2048]{1,0:T(8,128)(2,1)} %tokens_in.1, s32[2,128]{1,0:T(2,128)} %bitcast.3, f32[2,128]{1,0:T(2,128)} %bitcast.5, f32[1,256]{1,0:T(1,128)} %bitcast.6, ...), custom_call_target="tpu_custom_call" | custom-call | tf_op jit(solution)/shard_map/pallas_call | solution.py:431
  160.1 0.0 copy-done
  160.1 2.7 %shard_map.103 = (bf16[2,2048,256]{2,1,0:T(8,128)(2,1)}, bf16[2,2048,256]{2,1,0:T(8,128)(2,1)}, bf16[2,2048,256]{2,1,0:T(8,128)(2,1)}, bf16[128,512]{1,0:T(8,128)(2,1)}) custom-call(s32[2,128]{1,0:T(2,128)S(1)} %bitcast.4, bf16[4,256,128]{2,1,0:T(8,128)(2,1)S(1)} %get-tuple-element.8.ret, bf16[2,2048,256]{2,1,0:T(8,128)(2,1)S(1)} %get-tuple-element.9.gate, ...), custom_call_target="tpu_custom_call" | custom-call | tf_op jit(solution)/shard_map/pallas_call | solution.py:464
Async XLA Ops:
  0.6 159.5 %copy-start = (s32[128,2]{0,1:T(2,128)S(1)}, s32[128,2]{0,1:T(2,128)}, u32[]{:S(2)}) copy-start(s32[128,2]{0,1:T(2,128)} %param.8) | copy-start | bytes 3076

commit v4 on v3

--- a/solution.py
+++ b/solution.py
@@ -8,6 +8,7 @@
 from jax.sharding import PartitionSpec as P
 
 GROUPS = 4
+ORDER = ((('near', 'inner', 'outer'), ('inner', 'outer', 'near')), (('near', 'inner', 'outer'), ('inner', 'outer', 'near')), (('near', 'inner', 'outer'), ('inner', 'outer', 'near')), (('near', 'outer', 'inner'), ('near', 'outer', 'inner')))
 EPSILON = 1e-06
 MESH = pl.DeviceIdType.MESH
 PAIR_LAG, CREW_LAG = 1, 3
@@ -67,8 +68,24 @@
     crews = nt // 2 * width
     served = (gate_out, up_out, down_out)
 
-    def target(k):
-        return lax.rem(jnp.where(f < nf // 2, f + k, f + nf - k), nf)
+    lower = g < GROUPS // 2
+    outer = (g == 0) | (g == GROUPS - 1)
+    planes = {
+        "near": g ^ 1,
+        "inner": jnp.where(lower, GROUPS // 2, GROUPS // 2 - 1),
+        "outer": jnp.where(lower, GROUPS - 1, 0),
+    }
+
+    def pick(order, j):
+        first, second, third = (planes[name] for name in order)
+        return jnp.where(j == 0, first, jnp.where(j == 1, second, third))
+
+    def target(turn, k):
+        from_outer, from_inner = ORDER[turn]
+        j, r = k // width - 1, lax.rem(k, width)
+        z = jnp.where(outer, pick(from_outer, j), pick(from_inner, j))
+        x = lax.rem(m + r + 1, width) if turn == 3 else jnp.where(lower, r, width - 1 - r)
+        return jnp.where(k < width, g * width + lax.rem(m + k, width), z * width + x)
 
     def other(k):
         return lax.rem(t + k, nt)
@@ -83,7 +100,7 @@
         return pl.ds(pl.multiple_of(start * size, size), size)
 
     def loads(a, k):
-        p = target(k)
+        p = jnp.where(k == 0, f, target(a, k))
         return pltpu.make_async_copy(
             (gate, up, down)[a].at[pl.ds(p * per, per)],
             wf.at[a % 2, pl.ds(p * per, per)],
@@ -157,7 +174,7 @@
 
     barrier = pltpu.get_barrier_semaphore()
     each(1, nf, lambda k: pl.semaphore_signal(
-        barrier, inc=1, device_id={"fs": target(k)}, device_id_type=MESH))
+        barrier, inc=1, device_id={"fs": lax.rem(f + k, nf)}, device_id_type=MESH))
     each(1, nt, lambda k: pl.semaphore_signal(
         barrier, inc=1, device_id={"tp": other(k)}, device_id_type=MESH))
     inputs = [
@@ -217,7 +234,7 @@
                 loads(a + 1, k).start()
 
         def one(k):
-            p = target(k)
+            p = target(a, k)
             loads(a, k).wait()
             load_next(k)
             for e in range(per):
@@ -232,8 +249,7 @@
 
     def send_down(first, end):
         for h in range(first, end):
-            last = nf if h == parts - 1 else 0
-            each(1, nf, lambda k: down_copy(h, target(last - k if last else k), f).start())
+            each(1, nf, lambda k: down_copy(h, target(2 + (h > 0), k), f).start())
 
     with jax.named_scope('send0'):
         send_weights(0)
@@ -242,7 +258,6 @@
         send_weights(1)
     with jax.named_scope('send2'):
         send_weights(2)
-    outer = (g == 0) | (g == GROUPS - 1)
     pl.when(jnp.logical_not(outer))(lambda: send_down(0, parts))
 
     with jax.named_scope('arrive'):
@@ -299,13 +314,15 @@
     blocks = pieces // parts
     quarter = pieces // GROUPS
     wide_blocks = blocks // GROUPS
-    low = g < GROUPS // 2
-
     def piece_at(n):
-        i, r = n // quarter, lax.rem(n, quarter)
-        far = jnp.where(low, GROUPS + 1 - i, i - 2)
-        z = jnp.where(i < 2, g ^ i, far)
-        return (z * wide_blocks + lax.rem(r, wide_blocks)) * parts + r // wide_blocks
+        j, r = (n - quarter) // wide_blocks, lax.rem(n, wide_blocks)
+        first = n < quarter
+        h = jnp.where(first, n // wide_blocks, jnp.where(outer, lax.rem(j, parts), j // 3))
+        turn = jnp.where(outer, j // parts, lax.rem(j, 3))
+        turn = jnp.where((turn < 2) & (h > 0) & jnp.logical_not(outer), 1 - turn, turn)
+        far = jnp.where(lower, GROUPS - turn, turn - 1)
+        z = jnp.where(first, g, jnp.where(turn == 0, g ^ 1, far))
+        return (z * wide_blocks + r) * parts + h
 
     def multiply(n):
         c = piece_at(n)
@@ -347,23 +364,31 @@
         def _():
             ret[lax.rem(c, per_owner), span(g * split + rest, share), :] = rs[c]
 
-        @pl.when(jnp.logical_not(local))
+        pl.when(jnp.logical_not(crossing) | (n >= late) | (n < 0))(lambda: send_back(n))
+
+    crossing = outer & ((home < GROUPS // 2) != (g < GROUPS // 2))
+
+    def send_back(n):
+        c = piece_at(n)
+        owner = c // per_owner
+
+        @pl.when((home != g) | (owner != t))
         def _():
             return_copy(c, home * width + m, owner, g * split + rest).start()
 
+    late = pieces - wide_blocks
+
     def step(n):
-        @pl.when(n < pieces)
-        def _():
-            multiply(n)
-
-        @pl.when((n >= PAIR_LAG) & (n < pieces + PAIR_LAG))
-        def _():
-            reduce(n - PAIR_LAG)
-
-        @pl.when(n >= CREW_LAG)
-        def _():
-            give_back(n - CREW_LAG)
-    each(0, pieces + CREW_LAG, step)
+        multiply(n)
+        pl.when(n >= PAIR_LAG)(lambda: reduce(n - PAIR_LAG))
+        pl.when(n >= CREW_LAG)(lambda: give_back(n - CREW_LAG))
+    each(0, late, step)
+    each(late - PAIR_LAG, late, reduce)
+    each(late - CREW_LAG, late, give_back)
+    each(late, pieces, multiply)
+    each(late, pieces, reduce)
+    each(late, pieces, give_back)
+    pl.when(crossing)(lambda: each(0, late, send_back))
 
     own_share = pieces - per_owner
 

time: 164 us -> 161 us (0.982)
  Pallas kernels: 162 us -> 160 us
    pallas_call x1, Pallas kernels: 159 us -> 157 us  [body(): pl.pallas_call(functools.partial(kernel, nf, nt), out_shape=[pltpu.VMEM(s...]
where the time goes in v4:
time: 161 us
  Pallas kernels  160 us (99%)
    pallas_call x1, Pallas kernels, body(): pl.pallas_call(functools.partial(kernel, nf, nt), out_shape=[pltpu.VMEM(s...  157 us

profile of v4, /device:TPU:1, one launch (start us, length us, event | category | flops | bytes accessed | tf_op | source)
XLA Modules:
  0.0 160.9 jit_solution(12121636477532277983)
XLA Ops:
  0.6 0.0 copy-start
  0.6 157.5 %shard_map.102 = (bf16[2,2048,256]{2,1,0:T(8,128)(2,1)S(1)}, bf16[2,2048,256]{2,1,0:T(8,128)(2,1)S(1)}, bf16[2,2048,256]{2,1,0:T(8,128)(2,1)S(1)}, bf16[4,256,128]{2,1,0:T(8,128)(2,1)S(1)}) custom-call(bf16[128,2048]{1,0:T(8,128)(2,1)} %tokens_in.1, s32[2,128]{1,0:T(2,128)} %bitcast.3, f32[2,128]{1,0:T(2,128)} %bitcast.5, f32[1,256]{1,0:T(1,128)} %bitcast.6, ...), custom_call_target="tpu_custom_call" | custom-call | tf_op jit(solution)/shard_map/pallas_call | solution.py:456
  158.1 0.0 copy-done
  158.1 2.7 %shard_map.103 = (bf16[2,2048,256]{2,1,0:T(8,128)(2,1)}, bf16[2,2048,256]{2,1,0:T(8,128)(2,1)}, bf16[2,2048,256]{2,1,0:T(8,128)(2,1)}, bf16[128,512]{1,0:T(8,128)(2,1)}) custom-call(s32[2,128]{1,0:T(2,128)S(1)} %bitcast.4, bf16[4,256,128]{2,1,0:T(8,128)(2,1)S(1)} %get-tuple-element.8.ret, bf16[2,2048,256]{2,1,0:T(8,128)(2,1)S(1)} %get-tuple-element.9.gate, ...), custom_call_target="tpu_custom_call" | custom-call | tf_op jit(solution)/shard_map/pallas_call | solution.py:489
Async XLA Ops:
  0.6 157.5 %copy-start = (s32[128,2]{0,1:T(2,128)S(1)}, s32[128,2]{0,1:T(2,128)}, u32[]{:S(2)}) copy-start(s32[128,2]{0,1:T(2,128)} %param.8) | copy-start | bytes 3076

commit v5 on v4

--- a/solution.py
+++ b/solution.py
@@ -364,7 +364,7 @@
         def _():
             ret[lax.rem(c, per_owner), span(g * split + rest, share), :] = rs[c]
 
-        pl.when(jnp.logical_not(crossing) | (n >= late) | (n < 0))(lambda: send_back(n))
+        pl.when(jnp.logical_not(crossing) | (n >= late))(lambda: send_back(n))
 
     crossing = outer & ((home < GROUPS // 2) != (g < GROUPS // 2))
 
@@ -384,10 +384,9 @@
         pl.when(n >= CREW_LAG)(lambda: give_back(n - CREW_LAG))
     each(0, late, step)
     each(late - PAIR_LAG, late, reduce)
-    each(late - CREW_LAG, late, give_back)
     each(late, pieces, multiply)
     each(late, pieces, reduce)
-    each(late, pieces, give_back)
+    each(late - CREW_LAG, pieces, give_back)
     pl.when(crossing)(lambda: each(0, late, send_back))
 
     own_share = pieces - per_owner

time: 161 us -> 161 us (level)
  no operation moved by 1% of the time
where the time goes in v5:
time: 161 us; the launch traced here: 160 us
  Pallas kernels  160 us (99%)
    pallas_call x1, Pallas kernels, body(): pl.pallas_call(functools.partial(kernel, nf, nt), out_shape=[pltpu.VMEM(s...  157 us

profile of v5, /device:TPU:1, one launch (start us, length us, event | category | flops | bytes accessed | tf_op | source)
XLA Modules:
  0.0 160.4 jit_solution(17939647133444356268)
XLA Ops:
  0.6 0.0 copy-start
  0.6 157.0 %shard_map.102 = (bf16[2,2048,256]{2,1,0:T(8,128)(2,1)S(1)}, bf16[2,2048,256]{2,1,0:T(8,128)(2,1)S(1)}, bf16[2,2048,256]{2,1,0:T(8,128)(2,1)S(1)}, bf16[4,256,128]{2,1,0:T(8,128)(2,1)S(1)}) custom-call(bf16[128,2048]{1,0:T(8,128)(2,1)} %tokens_in.1, s32[2,128]{1,0:T(2,128)} %bitcast.3, f32[2,128]{1,0:T(2,128)} %bitcast.5, f32[1,256]{1,0:T(1,128)} %bitcast.6, ...), custom_call_target="tpu_custom_call" | custom-call | tf_op jit(solution)/shard_map/pallas_call | solution.py:455
  157.7 0.0 copy-done
  157.7 2.7 %shard_map.103 = (bf16[2,2048,256]{2,1,0:T(8,128)(2,1)}, bf16[2,2048,256]{2,1,0:T(8,128)(2,1)}, bf16[2,2048,256]{2,1,0:T(8,128)(2,1)}, bf16[128,512]{1,0:T(8,128)(2,1)}) custom-call(s32[2,128]{1,0:T(2,128)S(1)} %bitcast.4, bf16[4,256,128]{2,1,0:T(8,128)(2,1)S(1)} %get-tuple-element.8.ret, bf16[2,2048,256]{2,1,0:T(8,128)(2,1)S(1)} %get-tuple-element.9.gate, ...), custom_call_target="tpu_custom_call" | custom-call | tf_op jit(solution)/shard_map/pallas_call | solution.py:488
Async XLA Ops:
  0.6 157.0 %copy-start = (s32[128,2]{0,1:T(2,128)S(1)}, s32[128,2]{0,1:T(2,128)}, u32[]{:S(2)}) copy-start(s32[128,2]{0,1:T(2,128)} %param.8) | copy-start | bytes 3076
